TPU v7x, 512 devices: a whole 4x8x8 slice. The times are simulated.
512 devices in a mesh: sp: 32 (over z, x), tp: 16 (over y, core).
Axes of the slice: x: 4, y: 8, z: 8, core: 2. Of those that a mesh axis runs over, the one named last changes fastest.
Arguments:
- outer_gate: bfloat16 [8192, 2048], P('sp', 'tp'), may hold values from -6 to 6
- inner_gate: bfloat16 [8192, 2048], P('sp', 'tp'), may hold values from -6 to 6
- conv_input: bfloat16 [8192, 2048], P('sp', 'tp'), may hold values from -6 to 6
- conv_weight: bfloat16 [3, 2048], P(None, 'tp'), may hold values from -3.5 to 3.5
- doc_ids: int32 [8192], P('sp'), may hold values from 0 to 15, as said below
- output_weight: bfloat16 [2048, 4096], P(None, 'tp'), may hold values from -0.125 to 0.125
- residual: bfloat16 [8192, 4096], P('sp', 'tp'), as said below
- norm_gain: bfloat16 [4096], P('tp'), may hold values from 0.099609375 to 1.8984375
- expert_ids: int32 [8192, 2], P('sp'), may hold values from 0 to 31, all different within a row; in each aligned block of 256 rows (0 to 255, 256 to 511, ...) at most 32 rows name the same one
- group_weight: float32 [8192], P('sp'), may hold values from 0.25 to 1
- expert_weight: float32 [8192, 2], P('sp'), may hold values from 0.05 to 1
- gate_weight: bfloat16 [32, 4096, 2048], P('sp', None, 'tp'), may hold values from -0.09375 to 0.09375
- up_weight: bfloat16 [32, 4096, 2048], P('sp', None, 'tp'), may hold values from -0.09375 to 0.09375
- down_weight: bfloat16 [32, 2048, 4096], P('sp', None, 'tp'), may hold values from -0.125 to 0.125
Outputs:
- layer_out: bfloat16 [8192, 4096], P('sp', 'tp')
Inputs may be any that keep to these rules, and one draw needn't show every extreme that they name: `expert_ids`: within the 256 rows of one index of sp no expert is named more than 32 times, a bound that some block reaches; the two experts of a row differ. `doc_ids`: never falling along positions, rising by one at each document's start; every document has 256 to 768 positions, and one exactly 768. `residual`: Columns' scales are of order one to ten.
All inputs are finite; a program needn't handle non-finite values.
Results may differ from a plain program's by a relative error of at most 0.009.
Values may be sent and summed in bfloat16 or wider, within the bound.
A program may use at most 64 MiB of HBM per device.

v0:
```python
import jax
import jax.numpy as jnp
from jax import lax
from jax.sharding import PartitionSpec as P

EPS = 1e-06


def passed_along(value, axis, steps):
    count = lax.axis_size(axis)
    initial, last = (max(0, -steps), min(count, count - steps))
    return lax.ppermute(value, axis, [(source, source + steps) for source in range(initial, last)])


def from_everyone(x, axis):
    copies = jnp.broadcast_to(x, (lax.axis_size(axis), *x.shape))
    return lax.all_to_all(copies, axis, split_axis=0, concat_axis=0, tiled=True)


def joined_along(blocks, dim):
    dims = list(blocks.shape[1:])
    dims[dim] *= blocks.shape[0]
    return jnp.moveaxis(blocks, 0, dim).reshape(dims)


def collect(x, axis, dim):
    blocks = from_everyone(x, axis)
    return joined_along(blocks, dim)


def of_everyone(x, axis):
    everything = from_everyone(x, axis)
    return jnp.sum(everything, axis=0)


def per_device(
    outer_gate,
    inner_gate,
    conv_input,
    conv_weight,
    doc_ids,
    output_weight,
    residual,
    norm_gain,
    expert_ids,
    group_weight,
    expert_weight,
    gate_weight,
    up_weight,
    down_weight,
):
    row_count = conv_input.shape[0]
    products = inner_gate.astype(jnp.float32) * conv_input.astype(jnp.float32)
    own_docs = doc_ids.astype(jnp.float32)
    tail_rows, tail_docs = passed_along((products[-2:], own_docs[-2:]), "sp", 1)
    ext_products = jnp.concatenate([tail_rows, products], axis=0)
    ext_docs = jnp.concatenate([tail_docs, own_docs], axis=0)
    taps = conv_weight.astype(jnp.float32)
    conv = taps[2] * products
    for shift_by in (1, 2):
        first = 2 - shift_by
        same_doc = (ext_docs[first : first + row_count] == own_docs)[:, None]
        conv = conv + jnp.where(
            same_doc, taps[2 - shift_by] * ext_products[first : first + row_count], 0.0
        )
    branch = (outer_gate.astype(jnp.float32) * conv).astype(jnp.bfloat16)
    cols_local = output_weight.shape[1]
    branch_sum = jnp.dot(
        collect(branch, "tp", 1), output_weight, preferred_element_type=jnp.float32
    )
    resid = (residual.astype(jnp.float32) + branch_sum).astype(jnp.bfloat16)
    resid_wide = resid.astype(jnp.float32)
    total_sq = of_everyone(jnp.sum(resid_wide * resid_wide, axis=1), "tp")
    width = cols_local * lax.axis_size("tp")
    scale = lax.rsqrt(total_sq / width + EPS)[:, None]
    normed = (resid_wide * scale * norm_gain.astype(jnp.float32)).astype(jnp.bfloat16)
    experts = lax.axis_size("sp")
    capacity = 4 * row_count // experts
    flat_experts = expert_ids.reshape(-1)
    onehot = (flat_experts[:, None] == jnp.arange(experts, dtype=jnp.int32)[None, :]).astype(
        jnp.int32
    )
    slot_rank = jnp.sum((jnp.cumsum(onehot, axis=0) - onehot) * onehot, axis=1)
    slot_index = flat_experts * capacity + slot_rank
    token_of = jnp.arange(2 * row_count, dtype=jnp.int32) // 2
    token_table = jnp.full((experts * capacity,), row_count, jnp.int32).at[slot_index].set(token_of)
    gate_local = gate_weight[0]
    up_local = up_weight[0]
    arrived_rows = experts * capacity
    padded = jnp.concatenate([normed, jnp.zeros((1, cols_local), jnp.bfloat16)], axis=0)
    outgoing = padded[token_table].reshape(experts, capacity, cols_local)
    arrived = lax.all_to_all(outgoing, "sp", split_axis=0, concat_axis=0, tiled=True).reshape(
        arrived_rows, cols_local
    )
    piece = lax.all_gather(arrived, "tp", axis=1, tiled=True)
    gate_val = jnp.dot(piece, gate_local, preferred_element_type=jnp.float32)
    up_val = jnp.dot(piece, up_local, preferred_element_type=jnp.float32)
    hidden = (jax.nn.silu(gate_val) * up_val).astype(jnp.bfloat16)
    down_local = down_weight[0]
    expert_out = jnp.dot(
        lax.all_gather(hidden, "tp", axis=1, tiled=True),
        down_local,
        preferred_element_type=jnp.float32,
    ).astype(jnp.bfloat16)
    returned = lax.all_to_all(
        expert_out.reshape(experts, capacity, cols_local),
        "sp",
        split_axis=0,
        concat_axis=0,
        tiled=True,
    )
    picked = (
        returned.reshape(arrived_rows, cols_local)[slot_index]
        .reshape(row_count, 2, cols_local)
        .astype(jnp.float32)
    )
    mix_weight = (
        group_weight[:, None] * expert_weight / jnp.sum(expert_weight, axis=1, keepdims=True)
    )
    routed_sum = jnp.sum(picked * mix_weight[:, :, None], axis=1)
    return (resid_wide + routed_sum).astype(jnp.bfloat16)


def solution(mesh):
    return jax.shard_map(
        per_device,
        mesh=mesh,
        in_specs=(
            P("sp", "tp"),
            P("sp", "tp"),
            P("sp", "tp"),
            P(None, "tp"),
            P("sp"),
            P(None, "tp"),
            P("sp", "tp"),
            P("tp"),
            P("sp", None),
            P("sp"),
            P("sp", None),
            P("sp", None, "tp"),
            P("sp", None, "tp"),
            P("sp", None, "tp"),
        ),
        out_specs=P("sp", "tp"),
        check_vma=False,
    )
```

profile of v0, /device:TPU:1, one launch (start us, length us, event | category | flops | bytes accessed | tf_op | source)
XLA Modules:
  0.0 263.7 jit_solution(17630297964401948509)
XLA Ops:
  6.5 0.8 convert_element_type.60
  7.4 3.9 %collective-permute-start = (f32[2]{0:T(128)S(1)}, f32[2]{0:T(128)S(1)}, u32[]{:S(2)}, u32[]{:S(2)}) collective-permute-start(f32[2]{0:T(128)S(1)} %slice.34), channel_id=1, source_target_pairs={{0,16},{16,32},{32,48},{48,64},{64,80},{80,96},{96,112},{112,128},... | collective-permute-start | bytes 32 | tf_op jit(solution)/shard_map/ppermute | solution.py:12
  11.4 0.9 convert_multiply_fusion
  12.3 3.1 %collective-permute-start.1 = (f32[2,128]{1,0:T(2,128)S(1)}, f32[2,128]{1,0:T(2,128)S(1)}, u32[]{:S(2)}, u32[]{:S(2)}) collective-permute-start(f32[2,128]{1,0:T(2,128)S(1)} %slice.48), channel_id=1, source_target_pairs={{0,16},{16,32},{32,48},{48,64},{64,80},{80,96},{96,112},{112,128},... | collective-permute-start | bytes 3080 | tf_op jit(solution)/shard_map/ppermute | solution.py:12
  16.9 1.0 fusion.13
  18.0 1.1 broadcast_in_dim.44
  19.1 8.3 %all-to-all-start = ((bf16[16,256,128]{1,2,0:T(8,128)(2,1)}), bf16[16,256,128]{1,2,0:T(8,128)(2,1)S(1)}, u32[]{:S(2)}, u32[]{:S(2)}) async-start(bf16[16,256,128]{1,2,0:T(8,128)(2,1)} %broadcast_in_dim.44), calls=%async_computation | async-start | bytes 2097152 | tf_op jit(solution)/shard_map/all_to_all | solution.py:17
  27.5 0.8 copy.31
  28.6 1.2 reduce-window.6
  31.1 2.4 scatter_custom_fusion
  33.6 21.9 %all-to-all-done = bf16[16,256,128]{1,2,0:T(8,128)(2,1)S(1)} async-done(((bf16[16,256,128]{1,2,0:T(8,128)(2,1)}), bf16[16,256,128]{1,2,0:T(8,128)(2,1)S(1)}, u32[]{:S(2)}, u32[]{:S(2)}) %all-to-all-start) | async-done | bytes 1048608 | tf_op jit(solution)/shard_map/all_to_all | solution.py:17
  55.5 1.8 multiply_reduce_fusion.1
  57.9 3.4 %all-to-all-start.1 = ((f32[16,1,256]{2,1,0:T(1,128)}), f32[16,1,256]{2,1,0:T(1,128)S(1)}, u32[]{:S(2)}, u32[]{:S(2)}) async-start(f32[16,1,256]{2,1,0:T(1,128)} %broadcast_in_dim.45), calls=%async_computation.1 | async-start | bytes 32768 | tf_op jit(solution)/shard_map/all_to_all | solution.py:17
  62.0 6.6 %all-to-all-done.1 = f32[16,1,256]{2,1,0:T(1,128)S(1)} async-done(((f32[16,1,256]{2,1,0:T(1,128)}), f32[16,1,256]{2,1,0:T(1,128)S(1)}, u32[]{:S(2)}, u32[]{:S(2)}) %all-to-all-start.1) | async-done | bytes 16416 | tf_op jit(solution)/shard_map/all_to_all | solution.py:17
  68.8 3.9 %gather_fusion = bf16[1024,256]{1,0:T(8,128)(2,1)S(1)} fusion(bf16[257,256]{1,0:T(8,128)(2,1)S(1)} %concatenate.11, s32[1024]{0:T(1024)S(1)} %fusion.20), kind=kCustom, calls=%fused_computation | custom fusion | bytes 1052672 | tf_op jit(solution)/shard_map/gather | solution.py:91
  72.8 30.8 %all_to_all.21 = bf16[32,32,256]{2,1,0:T(8,128)(2,1)} all-to-all(bf16[32,32,256]{2,1,0:T(8,128)(2,1)S(1)} %bitcast.51), channel_id=1, replica_groups=mesh['sp'=32,'tp'=16] {'sp'}, dimensions={0} | all-to-all | bytes 1048576 | tf_op jit(solution)/shard_map/all_to_all | solution.py:92
  103.6 62.4 %all-gather.3.cloned.1.call-done = bf16[1024,4096]{1,0:T(8,128)(2,1)} async-done(((bf16[1024,256]{1,0:T(8,128)(2,1)}), bf16[1024,4096]{1,0:T(8,128)(2,1)}) %all-gather.3.cloned.1.call-update) | async-done | bytes 8388624 | tf_op jit(solution)/shard_map/all_gather | solution.py:95
  166.0 5.9 %fusion.5 = f32[1024,128]{1,0:T(8,128)S(1)} fusion(bf16[1024,4096]{1,0:T(8,128)(2,1)} %all-gather.3.cloned.1.call-done, bf16[1,4096,128]{2,1,0:T(8,128)(2,1)S(1)} %copy-done.4), kind=kOutput, calls=%fused_computation.11 | convolution fusion | flops 1073741824 | bytes 9961472 | tf_op jit(solution)/shard_map/dot_general | solution.py:96
  172.0 3.0 %fusion = bf16[1024,128]{1,0:T(8,128)(2,1)} fusion(bf16[1024,4096]{1,0:T(8,128)(2,1)S(1)} %copy-done.3, bf16[1,4096,128]{2,1,0:T(8,128)(2,1)S(1)} %copy-done.5, f32[1024,128]{1,0:T(8,128)S(1)} %fusion.5), kind=kOutput, calls=%fused_computation.5 | convolution fusion | flops 1074528256 | bytes 10223616 | tf_op jit(solution)/shard_map/dot_general | solution.py:97
  175.0 48.4 %all-gather.5.cloned.1.call-done = bf16[1024,2048]{1,0:T(8,128)(2,1)} async-done(((bf16[1024,128]{1,0:T(8,128)(2,1)}), bf16[1024,2048]{1,0:T(8,128)(2,1)}) %all-gather.5.cloned.1.call-update) | async-done | bytes 4194320 | tf_op jit(solution)/shard_map/all_gather | solution.py:101
  223.5 4.2 %convolution_convert_fusion = bf16[1024,256]{1,0:T(8,128)(2,1)} fusion(bf16[1024,2048]{1,0:T(8,128)(2,1)} %all-gather.5.cloned.1.call-done, bf16[1,2048,256]{2,1,0:T(8,128)(2,1)S(1)} %copy-done), kind=kOutput, calls=%fused_computation.3 | convolution fusion | flops 1074003968 | bytes 5767168 | tf_op jit(solution)/shard_map/dot_general | solution.py:100
  227.7 8.9 %all-to-all-start.3 = ((bf16[32,32,256]{2,1,0:T(8,128)(2,1)}), bf16[32,32,256]{2,1,0:T(8,128)(2,1)S(1)}, u32[]{:S(2)}, u32[]{:S(2)}) async-start(bf16[32,32,256]{2,1,0:T(8,128)(2,1)} %bitcast.13), calls=%async_computation.3 | async-start | bytes 1048576 | tf_op jit(solution)/shard_map/all_to_all | solution.py:105
  236.8 16.4 %all-to-all-done.3 = bf16[32,32,256]{2,1,0:T(8,128)(2,1)S(1)} async-done(((bf16[32,32,256]{2,1,0:T(8,128)(2,1)}), bf16[32,32,256]{2,1,0:T(8,128)(2,1)S(1)}, u32[]{:S(2)}, u32[]{:S(2)}) %all-to-all-start.3) | async-done | bytes 524320 | tf_op jit(solution)/shard_map/all_to_all | solution.py:105
  253.2 1.9 gather_fusion.1
  (51 shorter events, 6.9 us)
Async XLA Ops:
  6.5 216.9 %copy-start = (bf16[1,2048,256]{2,1,0:T(8,128)(2,1)S(1)}, bf16[1,2048,256]{2,1,0:T(8,128)(2,1)}, u32[]{:S(2)}) copy-start(bf16[1,2048,256]{2,1,0:T(8,128)(2,1)} %param.27) | copy-start | bytes 3145732
  6.5 159.5 %copy-start.4 = (bf16[1,4096,128]{2,1,0:T(8,128)(2,1)S(1)}, bf16[1,4096,128]{2,1,0:T(8,128)(2,1)}, u32[]{:S(2)}) copy-start(bf16[1,4096,128]{2,1,0:T(8,128)(2,1)} %param.25) | copy-start | bytes 3145732
  7.4 8.7 %collective-permute-start = (f32[2]{0:T(128)S(1)}, f32[2]{0:T(128)S(1)}, u32[]{:S(2)}, u32[]{:S(2)}) collective-permute-start(f32[2]{0:T(128)S(1)} %slice.34), channel_id=1, source_target_pairs={{0,16},{16,32},{32,48},{48,64},{64,80},{80,96},{96,112},{112,128},... | collective-permute-start | bytes 32 | tf_op jit(solution)/shard_map/ppermute | solution.py:12
  12.3 4.7 %collective-permute-start.1 = (f32[2,128]{1,0:T(2,128)S(1)}, f32[2,128]{1,0:T(2,128)S(1)}, u32[]{:S(2)}, u32[]{:S(2)}) collective-permute-start(f32[2,128]{1,0:T(2,128)S(1)} %slice.48), channel_id=1, source_target_pairs={{0,16},{16,32},{32,48},{48,64},{64,80},{80,96},{96,112},{112,128},... | collective-permute-start | bytes 3080 | tf_op jit(solution)/shard_map/ppermute | solution.py:12
  19.1 36.3 %all-to-all-start = ((bf16[16,256,128]{1,2,0:T(8,128)(2,1)}), bf16[16,256,128]{1,2,0:T(8,128)(2,1)S(1)}, u32[]{:S(2)}, u32[]{:S(2)}) async-start(bf16[16,256,128]{1,2,0:T(8,128)(2,1)} %broadcast_in_dim.44), calls=%async_computation | async-start | bytes 2097152 | tf_op jit(solution)/shard_map/all_to_all | solution.py:17
  57.9 10.8 %all-to-all-start.1 = ((f32[16,1,256]{2,1,0:T(1,128)}), f32[16,1,256]{2,1,0:T(1,128)S(1)}, u32[]{:S(2)}, u32[]{:S(2)}) async-start(f32[16,1,256]{2,1,0:T(1,128)} %broadcast_in_dim.45), calls=%async_computation.1 | async-start | bytes 32768 | tf_op jit(solution)/shard_map/all_to_all | solution.py:17
  61.3 104.7 %all-gather.3.cloned.1.call-start = ((), (), s32[]{:S(2)}) async-start(), calls=%async_computation.4 | async-start | bytes 8912896 | tf_op jit(solution)/shard_map/all_gather | solution.py:95
  103.6 119.9 %all-gather.5.cloned.1.call-start = ((), (), s32[]{:S(2)}) async-start(), calls=%async_computation.5 | async-start | bytes 4456448 | tf_op jit(solution)/shard_map/all_gather | solution.py:101
  166.0 5.9 %copy-start.3 = (bf16[1024,4096]{1,0:T(8,128)(2,1)S(1)}, bf16[1024,4096]{1,0:T(8,128)(2,1)}, u32[]{:S(2)}) copy-start(bf16[1024,4096]{1,0:T(8,128)(2,1)} %all-gather.3.cloned.1.call-done) | copy-start | bytes 25165828
  166.0 6.0 %copy-start.5 = (bf16[1,4096,128]{2,1,0:T(8,128)(2,1)S(1)}, bf16[1,4096,128]{2,1,0:T(8,128)(2,1)}, u32[]{:S(2)}) copy-start(bf16[1,4096,128]{2,1,0:T(8,128)(2,1)} %param.26) | copy-start | bytes 3145732
  172.0 64.6 %copy-start.1 = (f32[256,2]{0,1:T(2,128)S(1)}, f32[256,2]{0,1:T(2,128)}, u32[]{:S(2)}) copy-start(f32[256,2]{0,1:T(2,128)} %param.24) | copy-start | bytes 6148
  172.0 64.7 %copy-start.2 = (f32[256]{0:T(256)S(1)}, f32[256]{0:T(256)}, u32[]{:S(2)}) copy-start(f32[256]{0:T(256)} %param.23) | copy-start | bytes 3076
  227.7 25.5 %all-to-all-start.3 = ((bf16[32,32,256]{2,1,0:T(8,128)(2,1)}), bf16[32,32,256]{2,1,0:T(8,128)(2,1)S(1)}, u32[]{:S(2)}, u32[]{:S(2)}) async-start(bf16[32,32,256]{2,1,0:T(8,128)(2,1)} %bitcast.13), calls=%async_computation.3 | async-start | bytes 1048576 | tf_op jit(solution)/shard_map/all_to_all | solution.py:105
Sparse Core Ops, SparseCore 0:
  103.7 62.2 all-gather.2
  175.2 48.2 all-gather.4
where the time goes:
time: 264 us
  waiting for transfers between devices  156 us (59%)
  blocking collectives  30.8 us (12%)
  starting transfers between devices  27.8 us (11%)
  matrix products  14.9 us (6%)
  between operations  13.6 us (5%)
  local copies, waits for them, and re-layouts  12.4 us (5%)
  other arithmetic  8.46 us (3%)
    all_gather x1, waiting for transfers between devices, per_device(): piece = lax.all_gather(arrived, 'tp', axis=1, tiled=True)  62.4 us
    all_gather x1, waiting for transfers between devices, per_device(): lax.all_gather(hidden, 'tp', axis=1, tiled=True)  48.4 us
    all_to_all x1, blocking collectives, per_device(): lax.all_to_all(outgoing, 'sp', split_axis=0, concat_axis=0, tiled=True)  30.8 us
    all_to_all x2, waiting for transfers between devices, from_everyone(): return lax.all_to_all(copies, axis, split_axis=0, concat_axis=0, tiled=True)  28.5 us
    all_to_all x1, waiting for transfers between devices, per_device(): lax.all_to_all(expert_out.reshape(experts, capacity, cols_local), 'sp', s...  16.4 us
    all_to_all x2, starting transfers between devices, from_everyone(): return lax.all_to_all(copies, axis, split_axis=0, concat_axis=0, tiled=True)  11.8 us
    all_to_all x1, starting transfers between devices, per_device(): lax.all_to_all(expert_out.reshape(experts, capacity, cols_local), 'sp', s...  8.95 us
    ppermute x2, starting transfers between devices, passed_along(): lax.ppermute(value, axis, [(source, source + steps) for source in range(i...  7.04 us
  transfers between devices with their start and end apart: 7, of which 5 were waited for; matrix products, arithmetic and copies ran while one was open for 4% of the time, Pallas kernels for 0%

commit v1 on v0

v1 whole, which is shorter than its diff:
```python
import functools
import jax
import jax.numpy as jnp
from jax import lax
from jax.experimental import pallas as pl
from jax.experimental.pallas import tpu as pltpu
from jax.sharding import PartitionSpec as P

EPS = 1e-06
MESH = pl.DeviceIdType.MESH
F32 = jnp.float32
BF16 = jnp.bfloat16

SP, NX, NZ = 32, 4, 8
TP, NY = 16, 8
ROWS = 256
COLS = 256
CH = 128
CAP = 32
SLOTS = SP * CAP
PIECES = 4
PROWS = SLOTS // PIECES
BROWS = 288
BPIECES = 2
BPROWS = BROWS // BPIECES


def rdma(src, dst, ssem, rsem, dev):
    return pltpu.make_async_remote_copy(
        src_ref=src, dst_ref=dst, send_sem=ssem, recv_sem=rsem, device_id=dev, device_id_type=MESH
    )


class Ring:
    def __init__(self, buf, pieces, prows, rsem, dsem, ssem, s, y, c):
        self.buf, self.pieces, self.prows = buf, pieces, prows
        self.rsem, self.dsem, self.ssem = rsem, dsem, ssem
        self.s, self.y, self.c = s, y, c
        self.plus = (s, 2 * ((y + 1) % NY) + c)
        self.minus = (s, 2 * ((y + NY - 1) % NY) + c)
        self.partner = (s, 2 * y + (1 - c))

    def at(self, chunk, p):
        return self.buf.at[chunk, pl.ds(pl.multiple_of(p * self.prows, 16), self.prows)]

    def ring(self, origin, p, dev):
        ref = self.at(2 * origin + self.c, p)
        return rdma(ref, ref, self.ssem, self.rsem.at[origin, p], dev)

    def local(self, origin, core, p):
        ref = self.at(2 * origin + core, p)
        return rdma(ref, ref, self.ssem, self.dsem.at[origin, p], self.partner)

    def begin(self, p):
        self.ring(self.y, p, self.plus).start()
        self.ring(self.y, p, self.minus).start()
        self.local(self.y, self.c, p).start()

    def own(self, p, compute):
        compute(2 * self.y + self.c, p)

    def arrivals(self, k, p, compute):
        half = self.pieces // 2
        low, high = p < half, p >= half
        up = (self.y + NY - k) % NY
        down = (self.y + k) % NY
        c = self.c

        @pl.when((k < 4) | low)
        def _():
            self.ring(up, p, self.plus).wait_recv()

            @pl.when((k < 3) | ((k == 3) & low))
            def _():
                self.ring(up, p, self.plus).start()

            self.local(up, c, p).start()

        @pl.when((k < 4) | high)
        def _():
            self.ring(down, p, self.minus).wait_recv()

            @pl.when((k < 3) | ((k == 3) & high))
            def _():
                self.ring(down, p, self.minus).start()

            self.local(down, c, p).start()

        compute(2 * up + c, p)

        @pl.when(k < 4)
        def _():
            compute(2 * down + c, p)

        pup = (self.y + NY - (k - 1)) % NY
        pdown = (self.y + (k - 1)) % NY
        self.local(pup, 1 - c, p).wait_recv()
        compute(2 * pup + 1 - c, p)

        @pl.when(k > 1)
        def _():
            self.local(pdown, 1 - c, p).wait_recv()
            compute(2 * pdown + 1 - c, p)

    def steps(self, compute):
        n = self.pieces

        def body(j, carry):
            self.arrivals(1 + j // n, j % n, compute)
            return carry

        lax.fori_loop(0, 4 * n, body, 0)

    def last(self, p, compute):
        far = (self.y + 4) % NY
        self.local(far, 1 - self.c, p).wait_recv()
        compute(2 * far + 1 - self.c, p)

    def drain(self):
        ref = self.buf.at[0:15]
        pltpu.make_async_copy(ref, ref, self.ssem).wait()


def kernel(
    og, ig, ci, cw, docs, resin, gain, ids, gw, ew, wo_hbm, wg_hbm, wu_hbm, wd_hbm,
    out,
    wo, wgu, wd, wsem,
    ext_p, ext_d, halo_p, halo_d, hsem,
    bbuf, bacc, brs, bds, bss,
    resid, sel, pick0, pick1, mixw,
    send, esem, els,
    xbuf, xacc, ssum, xrs, xds, xss,
    hbuf, hacc, hrs, hds, hss,
    obuf, ret, osem, ols,
):
    s = lax.axis_index("sp")
    t = lax.axis_index("tp")
    y, c = t // 2, t % 2
    z, x = s // NX, s % NX
    nxt = (s + 1) % SP

    loads = [
        pltpu.make_async_copy(wo_hbm, wo, wsem.at[0]),
        pltpu.make_async_copy(wg_hbm, wgu.at[:, 0:CH], wsem.at[1]),
        pltpu.make_async_copy(wu_hbm, wgu.at[:, CH : 2 * CH], wsem.at[2]),
        pltpu.make_async_copy(wd_hbm, wd, wsem.at[3]),
    ]
    for load in loads:
        load.start()

    barrier = pltpu.get_barrier_semaphore()

    def greet(i, carry):
        pl.semaphore_signal(barrier, inc=1, device_id=((s + i) % SP, t), device_id_type=MESH)
        return carry

    lax.fori_loop(1, SP, greet, 0)
    for peer in (2 * ((y + 1) % NY) + c, 2 * ((y + NY - 1) % NY) + c, 2 * y + 1 - c):
        pl.semaphore_signal(barrier, inc=1, device_id=(s, peer), device_id_type=MESH)

    ext_p[8:264, :] = ig[...].astype(F32) * ci[...].astype(F32)
    id0, id1 = ids[0:1, :], ids[1:2, :]
    expert = lax.broadcasted_iota(jnp.int32, (SP, ROWS), 0)
    is0, is1 = expert == id0, expert == id1
    named = jnp.where(is0 | is1, 1.0, 0.0).astype(BF16)
    before = lax.broadcasted_iota(jnp.int32, (ROWS, ROWS), 0) < lax.broadcasted_iota(
        jnp.int32, (ROWS, ROWS), 1
    )
    ahead = jnp.dot(named, jnp.where(before, 1.0, 0.0).astype(BF16), preferred_element_type=F32)
    rank0 = jnp.sum(jnp.where(is0, ahead, 0.0), axis=0, keepdims=True)
    rank1 = jnp.sum(jnp.where(is1, ahead, 0.0), axis=0, keepdims=True)
    slot0 = id0.astype(F32) * CAP + rank0
    slot1 = id1.astype(F32) * CAP + rank1
    e0, e1 = ew[0:1, :], ew[1:2, :]
    esum = e0 + e1
    group = gw[...]
    table = jnp.concatenate(
        [
            docs[...].astype(F32),
            slot0,
            slot1,
            group * e0 / esum,
            group * e1 / esum,
            jnp.zeros((CH - 5, ROWS), F32),
        ],
        axis=0,
    )
    columns = table.T
    ext_d[8:264, :] = jnp.broadcast_to(columns[:, 0:1], (ROWS, CH))
    mixw[...] = columns

    pl.semaphore_wait(barrier, SP - 1 + 3)

    halos = [
        rdma(ext_p.at[256:264], halo_p, hsem.at[0], hsem.at[1], (nxt, t)),
        rdma(ext_d.at[256:264], halo_d, hsem.at[2], hsem.at[3], (nxt, t)),
    ]
    for halo in halos:
        halo.start()
    for halo in halos:
        halo.wait_recv()
    ext_p[0:8, :] = halo_p[...]
    ext_d[0:8, :] = halo_d[...]

    taps = cw[...].astype(F32)
    own_docs = ext_d[8:264, :]
    row = lax.broadcasted_iota(jnp.int32, (ROWS, CH), 0)
    conv = taps[2:3, :] * ext_p[8:264, :]
    for shift in (1, 2):
        same = (ext_d[8 - shift : 264 - shift, :] == own_docs) & ((row >= shift) | (s > 0))
        conv = conv + jnp.where(same, taps[2 - shift : 3 - shift, :] * ext_p[8 - shift : 264 - shift, :], 0.0)
    bbuf[t, 0:ROWS, :] = (og[...].astype(F32) * conv).astype(BF16)
    bbuf[t, ROWS:BROWS, :] = jnp.concatenate(
        [gain[...].astype(F32), jnp.zeros((BROWS - ROWS - 2, CH), F32)], axis=0
    ).astype(BF16)

    branch = Ring(bbuf, BPIECES, BPROWS, brs, bds, bss, s, y, c)
    for p in range(BPIECES):
        branch.begin(p)

    bacc[...] = jnp.zeros_like(bacc)
    loads[0].wait()

    def project(chunk, p):
        rows = pl.ds(pl.multiple_of(p * BPROWS, 16), BPROWS)
        weights = wo[pl.ds(pl.multiple_of(chunk * CH, CH), CH), :]
        bacc[rows, :] += jnp.dot(bbuf[chunk, rows, :], weights, preferred_element_type=F32)

    for p in range(BPIECES):
        branch.own(p, project)

    def tables(i, carry):
        rows = pl.ds(pl.multiple_of(i * 256, 256), 256)
        slot = (lax.broadcasted_iota(jnp.int32, (256, ROWS), 0) + i * 256).astype(F32)
        sel[rows, :] = jnp.where((slot == slot0) | (slot == slot1), 1.0, 0.0).astype(BF16)
        return carry

    lax.fori_loop(0, SLOTS // 256, tables, 0)

    branch.steps(project)
    for p in range(BPIECES):
        branch.last(p, project)

    resid[...] = (resin[...].astype(F32) + bacc[0:ROWS, :]).astype(BF16)

    def group_rows(i, carry):
        rows = pl.ds(pl.multiple_of(i * 256, 256), 256)
        send[rows, :] = jnp.dot(sel[rows, :], resid[...], preferred_element_type=F32).astype(BF16)
        return carry

    lax.fori_loop(0, SLOTS // 256, group_rows, 0)

    def place(p, d_z, d_x):
        return p * 8 + (d_z // 2) * 2 + d_x // 2

    def partners(p):
        px, pz = p // 2, p % 2
        for zh in (2, 1, 3, 0):
            for xh in (1, 0):
                yield (px, pz, zh, xh), (z + pz + 2 * zh) % NZ, (x + px + 2 * xh) % NX

    def block(ref, i):
        return ref.at[pl.ds(pl.multiple_of(i * CAP, CAP), CAP)]

    for p in range(PIECES):
        mine = place(p, z, x)
        for which, dz, dx in partners(p):
            d = dz * NX + dx
            dst = block(xbuf.at[t], mine)
            if which == (0, 0, 0, 0):
                pltpu.make_async_copy(block(send, d), dst, els.at[0]).start()
            else:
                rdma(block(send, d), dst, esem.at[SP], esem.at[mine], (d, t)).start()

    xacc[...] = jnp.zeros_like(xacc)
    ssum[...] = jnp.zeros_like(ssum)
    hacc[...] = jnp.zeros_like(hacc)
    for load in loads[1:3]:
        load.wait()

    def prows(p):
        return pl.ds(pl.multiple_of(p * PROWS, PROWS), PROWS)

    def widen(chunk, p):
        rows = prows(p)
        gains = bbuf[chunk, pl.ds(ROWS, 16), :].astype(F32)
        part = xbuf[chunk, rows, :].astype(F32)
        left, right = part[:, :CH], part[:, CH:]
        ssum[rows, :] += left * left + right * right
        scaled = jnp.concatenate([left * gains[0:1, :], right * gains[1:2, :]], axis=1).astype(BF16)
        weights = wgu[pl.ds(pl.multiple_of(chunk * COLS, COLS), COLS), :]
        xacc[rows, :] += jnp.dot(scaled, weights, preferred_element_type=F32)

    wide = Ring(xbuf, PIECES, PROWS, xrs, xds, xss, s, y, c)
    for p in range(PIECES):
        for which, dz, dx in partners(p):
            src = place(p, dz, dx)
            dst = block(xbuf.at[t], src)
            if which == (0, 0, 0, 0):
                pltpu.make_async_copy(dst, dst, els.at[0]).wait()
            else:
                rdma(dst, dst, esem.at[SP], esem.at[src], (s, t)).wait_recv()
        wide.begin(p)

    def own_rows(p, carry):
        wide.own(p, widen)
        return carry

    lax.fori_loop(0, PIECES, own_rows, 0)

    slot_lane = lax.broadcasted_iota(jnp.int32, (ROWS, SLOTS), 1).astype(F32)
    pick0[...] = jnp.where(slot_lane == mixw[:, 1:2], 1.0, 0.0).astype(BF16)
    pick1[...] = jnp.where(slot_lane == mixw[:, 2:3], 1.0, 0.0).astype(BF16)

    wide.steps(widen)

    deep = Ring(hbuf, PIECES, PROWS, hrs, hds, hss, s, y, c)

    def finish(p, carry):
        wide.last(p, widen)
        rows = prows(p)
        mean = jnp.sum(ssum[rows, :], axis=1, keepdims=True) / (TP * COLS)
        scale = lax.rsqrt(mean + EPS)
        gate = xacc[rows, 0:CH] * scale
        up = xacc[rows, CH : 2 * CH] * scale
        hbuf[t, rows, :] = (gate * jax.nn.sigmoid(gate) * up).astype(BF16)
        deep.begin(p)
        return carry

    lax.fori_loop(0, PIECES, finish, 0)
    loads[3].wait()

    def lower(chunk, p):
        rows = prows(p)
        weights = wd[pl.ds(pl.multiple_of(chunk * CH, CH), CH), :]
        hacc[rows, :] += jnp.dot(hbuf[chunk, rows, :], weights, preferred_element_type=F32)

    def own_hidden(p, carry):
        deep.own(p, lower)
        return carry

    lax.fori_loop(0, PIECES, own_hidden, 0)
    deep.steps(lower)

    for p in range(PIECES):
        deep.last(p, lower)
        rows = slice(p * PROWS, (p + 1) * PROWS)
        obuf[rows, :] = hacc[rows, :].astype(BF16)
        for which, dz, dx in partners(p):
            d = dz * NX + dx
            src = block(obuf, place(p, dz, dx))
            if which == (0, 0, 0, 0):
                pltpu.make_async_copy(src, block(ret, s), ols.at[0]).start()
            else:
                rdma(src, block(ret, s), osem.at[SP], osem.at[s], (d, t)).start()

    def arrive(i, carry):
        d = (s + i) % SP
        rdma(block(ret, d), block(ret, d), osem.at[SP], osem.at[d], (s, t)).wait_recv()
        return carry

    pltpu.make_async_copy(block(ret, s), block(ret, s), ols.at[0]).wait()
    lax.fori_loop(1, SP, arrive, 0)

    got0 = jnp.dot(pick0[...], ret[...], preferred_element_type=F32)
    got1 = jnp.dot(pick1[...], ret[...], preferred_element_type=F32)
    routed = got0 * mixw[:, 3:4] + got1 * mixw[:, 4:5]
    out[...] = (resid[...].astype(F32) + routed).astype(BF16)

    for halo in halos:
        halo.wait_send()
    branch.drain()
    rest = send.at[0 : SLOTS - CAP]
    pltpu.make_async_copy(rest, rest, esem.at[SP]).wait()
    wide.drain()
    deep.drain()
    rest = obuf.at[0 : SLOTS - CAP]
    pltpu.make_async_copy(rest, rest, osem.at[SP]).wait()


def per_device(
    outer_gate, inner_gate, conv_input, conv_weight, doc_ids, output_weight, residual,
    norm_gain, expert_ids, group_weight, expert_weight, gate_weight, up_weight, down_weight,
):
    dma = pltpu.SemaphoreType.DMA
    vmem = pl.BlockSpec(memory_space=pltpu.VMEM)
    hbm = pl.BlockSpec(memory_space=pl.ANY)
    scratch = [
        pltpu.VMEM((TP * CH, COLS), BF16),
        pltpu.VMEM((TP * COLS, 2 * CH), BF16),
        pltpu.VMEM((TP * CH, COLS), BF16),
        dma((4,)),
        pltpu.VMEM((264, CH), F32),
        pltpu.VMEM((264, CH), F32),
        pltpu.VMEM((8, CH), F32),
        pltpu.VMEM((8, CH), F32),
        dma((4,)),
        pltpu.VMEM((TP, BROWS, CH), BF16),
        pltpu.VMEM((BROWS, COLS), F32),
        dma((NY, BPIECES)),
        dma((NY, BPIECES)),
        dma,
        pltpu.VMEM((ROWS, COLS), BF16),
        pltpu.VMEM((SLOTS, ROWS), BF16),
        pltpu.VMEM((ROWS, SLOTS), BF16),
        pltpu.VMEM((ROWS, SLOTS), BF16),
        pltpu.VMEM((ROWS, CH), F32),
        pltpu.VMEM((SLOTS, COLS), BF16),
        dma((SP + 1,)),
        dma((1,)),
        pltpu.VMEM((TP, SLOTS, COLS), BF16),
        pltpu.VMEM((SLOTS, 2 * CH), F32),
        pltpu.VMEM((SLOTS, CH), F32),
        dma((NY, PIECES)),
        dma((NY, PIECES)),
        dma,
        pltpu.VMEM((TP, SLOTS, CH), BF16),
        pltpu.VMEM((SLOTS, COLS), F32),
        dma((NY, PIECES)),
        dma((NY, PIECES)),
        dma,
        pltpu.VMEM((SLOTS, COLS), BF16),
        pltpu.VMEM((SLOTS, COLS), BF16),
        dma((SP + 1,)),
        dma((1,)),
    ]
    return pl.pallas_call(
        kernel,
        name="layer",
        out_shape=jax.ShapeDtypeStruct((ROWS, COLS), BF16),
        in_specs=[vmem] * 10 + [hbm] * 4,
        out_specs=vmem,
        scratch_shapes=scratch,
        compiler_params=pltpu.CompilerParams(
            collective_id=0, has_side_effects=True, vmem_limit_bytes=56 * 1024 * 1024
        ),
    )(
        outer_gate,
        inner_gate,
        conv_input,
        conv_weight,
        doc_ids.reshape(1, ROWS),
        residual,
        norm_gain.reshape(2, CH),
        expert_ids.T,
        group_weight.reshape(1, ROWS),
        expert_weight.T,
        output_weight,
        gate_weight[0],
        up_weight[0],
        down_weight[0],
    )


def solution(mesh):
    return jax.shard_map(
        per_device,
        mesh=mesh,
        in_specs=(
            P("sp", "tp"),
            P("sp", "tp"),
            P("sp", "tp"),
            P(None, "tp"),
            P("sp"),
            P(None, "tp"),
            P("sp", "tp"),
            P("tp"),
            P("sp", None),
            P("sp"),
            P("sp", None),
            P("sp", None, "tp"),
            P("sp", None, "tp"),
            P("sp", None, "tp"),
        ),
        out_specs=P("sp", "tp"),
        check_vma=False,
    )
```

time: 264 us -> 128 us (0.48)
  waiting for transfers between devices: 156 us -> 0 us
  Pallas kernels: 0 us -> 125 us
  blocking collectives: 30.8 us -> 0 us
  starting transfers between devices: 27.8 us -> 0 us
  matrix products: 14.9 us -> 0 us
  between operations: 13.6 us -> 0.01 us
  local copies, waits for them, and re-layouts: 12.4 us -> 1.57 us
  other arithmetic: 8.46 us -> 0 us
    pallas_call x0 -> x1, Pallas kernels: none -> 125 us  [per_device(): pl.pallas_call(kernel, name='layer', out_shape=jax.ShapeDtypeStruct((ROWS...]
    all_gather x2 -> x0, waiting for transfers between devices: 111 us -> none  [the longest x1 62.4 us: per_device(): piece = lax.all_gather(arrived, 'tp', axis=1, tiled=True)]
    all_to_all x3 -> x0, waiting for transfers between devices: 44.9 us -> none  [the longest x2 28.5 us: from_everyone(): return lax.all_to_all(copies, axis, split_axis=0, concat_axis=0, tiled=True)]
    all_to_all x1 -> x0, blocking collectives: 30.8 us -> none  [per_device(): lax.all_to_all(outgoing, 'sp', split_axis=0, concat_axis=0, tiled=True)]
    all_to_all x3 -> x0, starting transfers between devices: 20.7 us -> none  [the longest x2 11.8 us: from_everyone(): return lax.all_to_all(copies, axis, split_axis=0, concat_axis=0, tiled=True)]
    dot_general x4 -> x0, matrix products: 14.9 us -> none  [the longest x1 5.86 us: per_device(): gate_val = jnp.dot(piece, gate_local, preferred_element_type=jnp.float32)]
    ppermute x2 -> x0, starting transfers between devices: 7.04 us -> none  [passed_along(): lax.ppermute(value, axis, [(source, source + steps) for source in range(i...]
    gather x2 -> x0, local copies, waits for them, and re-layouts: 5.89 us -> none  [the longest x1 3.94 us: per_device(): outgoing = padded[token_table].reshape(experts, capacity, cols_local)]
  transfers between devices with their start and end apart: 7 -> 0, of which waited for: 5 -> 0; matrix products, arithmetic and copies ran while one was open for 4% -> 0% of each run, Pallas kernels for 0% -> 0%
where the time goes in v1:
time: 128 us; the launch traced here: 126 us
  Pallas kernels  125 us (98%)
  local copies, waits for them, and re-layouts  1.57 us (1%)
    pallas_call x1, Pallas kernels, per_device(): pl.pallas_call(kernel, name='layer', out_shape=jax.ShapeDtypeStruct((ROWS...  125 us

profile of v1, /device:TPU:1, one launch (start us, length us, event | category | flops | bytes accessed | tf_op | source)
XLA Modules:
  0.0 126.5 jit_solution(3662449696861912234)
XLA Ops:
  0.0 124.9 %layer.1 = bf16[256,256]{1,0:T(8,128)(2,1)} custom-call(bf16[256,128]{1,0:T(8,128)(2,1)} %og.1, bf16[256,128]{1,0:T(8,128)(2,1)} %ig.1, bf16[256,128]{1,0:T(8,128)(2,1)} %ci.1, bf16[3,128]{1,0:T(4,128)(2,1)} %cw.1, s32[1,256]{1,0:T(1,128)} %bitcast.13, bf16[256,256]{1,0:T(8,128)(2,1)} %resin.1, bf16[2,128]{1,0:T(2,128)(2,1)} %bitcast.15, s32[2,256]{1,0:T(2,128)} %bitcast.11, ...), custom_call_target="tpu_custom_call" | custom-call | tf_op jit(solution)/shard_map/layer/pallas_call | solution.py:427
  124.9 1.6 %copy.16 = bf16[256,256]{1,0:T(8,128)(2,1)} copy(bf16[256,256]{1,0:T(8,128)(2,1)} %layer.1) | data formatting | bytes 262144

commit v2 on v1

--- a/solution.py
+++ b/solution.py
@@ -20,9 +20,11 @@
 SLOTS = SP * CAP
 PIECES = 4
 PROWS = SLOTS // PIECES
-BROWS = 288
-BPIECES = 2
-BPROWS = BROWS // BPIECES
+PER = SP // PIECES
+DELAY = (1, 1)
+ZORDER = (0, 1, 6, 3, 5, 4, 7, 2)
+BROWS = 272
+BSPLIT = ((0, 128), (128, 128), (256, 16))
 
 
 def rdma(src, dst, ssem, rsem, dev):
@@ -60,8 +62,7 @@
         compute(2 * self.y + self.c, p)
 
     def arrivals(self, k, p, compute):
-        half = self.pieces // 2
-        low, high = p < half, p >= half
+        low, high = p % 2 == 0, p % 2 == 1
         up = (self.y + NY - k) % NY
         down = (self.y + k) % NY
         c = self.c
@@ -101,15 +102,6 @@
         def _():
             self.local(pdown, 1 - c, p).wait_recv()
             compute(2 * pdown + 1 - c, p)
-
-    def steps(self, compute):
-        n = self.pieces
-
-        def body(j, carry):
-            self.arrivals(1 + j // n, j % n, compute)
-            return carry
-
-        lax.fori_loop(0, 4 * n, body, 0)
 
     def last(self, p, compute):
         far = (self.y + 4) % NY
@@ -128,10 +120,10 @@
     ext_p, ext_d, halo_p, halo_d, hsem,
     bbuf, bacc, brs, bds, bss,
     resid, sel, pick0, pick1, mixw,
-    send, esem, els,
+    send, esem,
     xbuf, xacc, ssum, xrs, xds, xss,
     hbuf, hacc, hrs, hds, hss,
-    obuf, ret, osem, ols,
+    obuf, ret, osem,
 ):
     s = lax.axis_index("sp")
     t = lax.axis_index("tp")
@@ -155,8 +147,10 @@
         return carry
 
     lax.fori_loop(1, SP, greet, 0)
-    for peer in (2 * ((y + 1) % NY) + c, 2 * ((y + NY - 1) % NY) + c, 2 * y + 1 - c):
+    for off in (1, 2, NY - 1, NY - 2):
+        peer = 2 * ((y + off) % NY) + c
         pl.semaphore_signal(barrier, inc=1, device_id=(s, peer), device_id_type=MESH)
+    pl.semaphore_signal(barrier, inc=1, device_id=(s, 2 * y + 1 - c), device_id_type=MESH)
 
     ext_p[8:264, :] = ig[...].astype(F32) * ci[...].astype(F32)
     id0, id1 = ids[0:1, :], ids[1:2, :]
@@ -189,7 +183,26 @@
     ext_d[8:264, :] = jnp.broadcast_to(columns[:, 0:1], (ROWS, CH))
     mixw[...] = columns
 
-    pl.semaphore_wait(barrier, SP - 1 + 3)
+    taps = cw[...].astype(F32)
+
+    def branch_rows(lo, hi):
+        own_docs = ext_d[8 + lo : 8 + hi, :]
+        row = lax.broadcasted_iota(jnp.int32, (hi - lo, CH), 0) + lo
+        conv = taps[2:3, :] * ext_p[8 + lo : 8 + hi, :]
+        for shift in (1, 2):
+            rows = slice(8 + lo - shift, 8 + hi - shift)
+            same = (ext_d[rows, :] == own_docs) & ((row >= shift) | (s > 0))
+            conv = conv + jnp.where(same, taps[2 - shift : 3 - shift, :] * ext_p[rows, :], 0.0)
+        return (og[lo:hi, :].astype(F32) * conv).astype(BF16)
+
+    bbuf[t, 0:128, :] = branch_rows(128, 256)
+    bbuf[t, 128:240, :] = branch_rows(16, 128)
+    bbuf[t, 240:256, :] = jnp.concatenate(
+        [gain[...].astype(F32), jnp.zeros((14, CH), F32)], axis=0
+    ).astype(BF16)
+    bacc[...] = jnp.zeros_like(bacc)
+
+    pl.semaphore_wait(barrier, SP - 1 + 5)
 
     halos = [
         rdma(ext_p.at[256:264], halo_p, hsem.at[0], hsem.at[1], (nxt, t)),
@@ -197,37 +210,62 @@
     ]
     for halo in halos:
         halo.start()
+
+    def near(off):
+        return (y + off + NY) % NY
+
+    def hop(origin, p, off):
+        lo, size = BSPLIT[p]
+        ref = bbuf.at[2 * origin + c, pl.ds(lo, size)]
+        return rdma(ref, ref, bss, brs.at[origin, p], (s, 2 * near(off) + c))
+
+    def across(origin, core, p):
+        lo, size = BSPLIT[p]
+        ref = bbuf.at[2 * origin + core, pl.ds(lo, size)]
+        return rdma(ref, ref, bss, bds.at[origin, p], (s, 2 * y + 1 - c))
+
+    def open_piece(p):
+        for off in (2, -2, 1, -1):
+            hop(y, p, off).start()
+        across(y, c, p).start()
+
+    open_piece(0)
+    open_piece(1)
     for halo in halos:
         halo.wait_recv()
     ext_p[0:8, :] = halo_p[...]
     ext_d[0:8, :] = halo_d[...]
-
-    taps = cw[...].astype(F32)
-    own_docs = ext_d[8:264, :]
-    row = lax.broadcasted_iota(jnp.int32, (ROWS, CH), 0)
-    conv = taps[2:3, :] * ext_p[8:264, :]
-    for shift in (1, 2):
-        same = (ext_d[8 - shift : 264 - shift, :] == own_docs) & ((row >= shift) | (s > 0))
-        conv = conv + jnp.where(same, taps[2 - shift : 3 - shift, :] * ext_p[8 - shift : 264 - shift, :], 0.0)
-    bbuf[t, 0:ROWS, :] = (og[...].astype(F32) * conv).astype(BF16)
-    bbuf[t, ROWS:BROWS, :] = jnp.concatenate(
-        [gain[...].astype(F32), jnp.zeros((BROWS - ROWS - 2, CH), F32)], axis=0
-    ).astype(BF16)
-
-    branch = Ring(bbuf, BPIECES, BPROWS, brs, bds, bss, s, y, c)
-    for p in range(BPIECES):
-        branch.begin(p)
-
-    bacc[...] = jnp.zeros_like(bacc)
+    bbuf[t, 256:272, :] = branch_rows(0, 16)
+    open_piece(2)
+
+    def far_side(p):
+        return 1 if p != 1 else -1
+
+    for p in range(3):
+        for side in (1, -1):
+            origin = near(-2 * side)
+            hop(origin, p, side).wait_recv()
+            if far_side(p) == side:
+                hop(origin, p, 2 * side).start()
+            hop(origin, p, side).start()
+            across(origin, c, p).start()
+        for side in (1, -1):
+            origin = near(-side)
+            hop(origin, p, side).wait_recv()
+            across(origin, c, p).start()
+
     loads[0].wait()
 
-    def project(chunk, p):
-        rows = pl.ds(pl.multiple_of(p * BPROWS, 16), BPROWS)
-        weights = wo[pl.ds(pl.multiple_of(chunk * CH, CH), CH), :]
-        bacc[rows, :] += jnp.dot(bbuf[chunk, rows, :], weights, preferred_element_type=F32)
-
-    for p in range(BPIECES):
-        branch.own(p, project)
+    def project(first, count, core):
+        def one(i, carry):
+            chunk = 2 * ((y + first + i) % NY) + core
+            weights = wo[pl.ds(pl.multiple_of(chunk * CH, CH), CH), :]
+            bacc[...] += jnp.dot(bbuf[chunk], weights, preferred_element_type=F32)
+            return carry
+
+        lax.fori_loop(0, count, one, 0)
+
+    project(6, 5, c)
 
     def tables(i, carry):
         rows = pl.ds(pl.multiple_of(i * 256, 256), 256)
@@ -237,11 +275,24 @@
 
     lax.fori_loop(0, SLOTS // 256, tables, 0)
 
-    branch.steps(project)
-    for p in range(BPIECES):
-        branch.last(p, project)
-
-    resid[...] = (resin[...].astype(F32) + bacc[0:ROWS, :]).astype(BF16)
+    for off in (3, -3, 4):
+        origin = near(off)
+        for p in range(3):
+            hop(origin, p, 1).wait_recv()
+            across(origin, c, p).start()
+    for off in (0, 1, -1, 2, -2):
+        for p in range(3):
+            across(near(off), 1 - c, p).wait_recv()
+    project(6, 5, 1 - c)
+    project(3, 3, c)
+    for off in (3, -3, 4):
+        for p in range(3):
+            across(near(off), 1 - c, p).wait_recv()
+    project(3, 3, 1 - c)
+
+    for (lo, size), first in zip(((0, 128), (128, 112), (256, 16)), (128, 16, 0)):
+        rows = slice(first, first + size)
+        resid[rows, :] = (resin[rows, :].astype(F32) + bacc[lo : lo + size, :]).astype(BF16)
 
     def group_rows(i, carry):
         rows = pl.ds(pl.multiple_of(i * 256, 256), 256)
@@ -250,32 +301,24 @@
 
     lax.fori_loop(0, SLOTS // 256, group_rows, 0)
 
-    def place(p, d_z, d_x):
-        return p * 8 + (d_z // 2) * 2 + d_x // 2
-
-    def partners(p):
-        px, pz = p // 2, p % 2
-        for zh in (2, 1, 3, 0):
-            for xh in (1, 0):
-                yield (px, pz, zh, xh), (z + pz + 2 * zh) % NZ, (x + px + 2 * xh) % NX
-
     def block(ref, i):
         return ref.at[pl.ds(pl.multiple_of(i * CAP, CAP), CAP)]
 
-    for p in range(PIECES):
-        mine = place(p, z, x)
-        for which, dz, dx in partners(p):
-            d = dz * NX + dx
-            dst = block(xbuf.at[t], mine)
-            if which == (0, 0, 0, 0):
-                pltpu.make_async_copy(block(send, d), dst, els.at[0]).start()
-            else:
-                rdma(block(send, d), dst, esem.at[SP], esem.at[mine], (d, t)).start()
+    def offsets(q):
+        return ZORDER[q // NX], q % NX
+
+    for q in range(SP):
+        dz, dx = offsets(q)
+        d = ((z + dz) % NZ) * NX + (x + dx) % NX
+        if q == 0:
+            pltpu.make_async_copy(block(send, d), block(xbuf.at[t], q), esem.at[q]).start()
+        else:
+            rdma(block(send, d), block(xbuf.at[t], q), esem.at[SP], esem.at[q], (d, t)).start()
 
     xacc[...] = jnp.zeros_like(xacc)
     ssum[...] = jnp.zeros_like(ssum)
     hacc[...] = jnp.zeros_like(hacc)
-    for load in loads[1:3]:
+    for load in loads[1:]:
         load.wait()
 
     def prows(p):
@@ -283,7 +326,7 @@
 
     def widen(chunk, p):
         rows = prows(p)
-        gains = bbuf[chunk, pl.ds(ROWS, 16), :].astype(F32)
+        gains = bbuf[chunk, pl.ds(240, 16), :].astype(F32)
         part = xbuf[chunk, rows, :].astype(F32)
         left, right = part[:, :CH], part[:, CH:]
         ssum[rows, :] += left * left + right * right
@@ -291,32 +334,30 @@
         weights = wgu[pl.ds(pl.multiple_of(chunk * COLS, COLS), COLS), :]
         xacc[rows, :] += jnp.dot(scaled, weights, preferred_element_type=F32)
 
-    wide = Ring(xbuf, PIECES, PROWS, xrs, xds, xss, s, y, c)
-    for p in range(PIECES):
-        for which, dz, dx in partners(p):
-            src = place(p, dz, dx)
-            dst = block(xbuf.at[t], src)
-            if which == (0, 0, 0, 0):
-                pltpu.make_async_copy(dst, dst, els.at[0]).wait()
-            else:
-                rdma(dst, dst, esem.at[SP], esem.at[src], (s, t)).wait_recv()
-        wide.begin(p)
-
-    def own_rows(p, carry):
-        wide.own(p, widen)
-        return carry
-
-    lax.fori_loop(0, PIECES, own_rows, 0)
+    def lower(chunk, p):
+        rows = prows(p)
+        weights = wd[pl.ds(pl.multiple_of(chunk * CH, CH), CH), :]
+        hacc[rows, :] += jnp.dot(hbuf[chunk, rows, :], weights, preferred_element_type=F32)
 
     slot_lane = lax.broadcasted_iota(jnp.int32, (ROWS, SLOTS), 1).astype(F32)
     pick0[...] = jnp.where(slot_lane == mixw[:, 1:2], 1.0, 0.0).astype(BF16)
     pick1[...] = jnp.where(slot_lane == mixw[:, 2:3], 1.0, 0.0).astype(BF16)
 
-    wide.steps(widen)
-
+    wide = Ring(xbuf, PIECES, PROWS, xrs, xds, xss, s, y, c)
     deep = Ring(hbuf, PIECES, PROWS, hrs, hds, hss, s, y, c)
 
-    def finish(p, carry):
+    def enter(p):
+        def one(i, carry):
+            q = p * PER + i
+            dst = block(xbuf.at[t], q)
+            pltpu.make_async_copy(dst, dst, esem.at[q]).wait()
+            return carry
+
+        lax.fori_loop(0, PER, one, 0)
+        wide.begin(p)
+        wide.own(p, widen)
+
+    def activate(p):
         wide.last(p, widen)
         rows = prows(p)
         mean = jnp.sum(ssum[rows, :], axis=1, keepdims=True) / (TP * COLS)
@@ -325,51 +366,65 @@
         up = xacc[rows, CH : 2 * CH] * scale
         hbuf[t, rows, :] = (gate * jax.nn.sigmoid(gate) * up).astype(BF16)
         deep.begin(p)
-        return carry
-
-    lax.fori_loop(0, PIECES, finish, 0)
-    loads[3].wait()
-
-    def lower(chunk, p):
-        rows = prows(p)
-        weights = wd[pl.ds(pl.multiple_of(chunk * CH, CH), CH), :]
-        hacc[rows, :] += jnp.dot(hbuf[chunk, rows, :], weights, preferred_element_type=F32)
-
-    def own_hidden(p, carry):
         deep.own(p, lower)
-        return carry
-
-    lax.fori_loop(0, PIECES, own_hidden, 0)
-    deep.steps(lower)
-
-    for p in range(PIECES):
+
+    def leave(p):
         deep.last(p, lower)
         rows = slice(p * PROWS, (p + 1) * PROWS)
         obuf[rows, :] = hacc[rows, :].astype(BF16)
-        for which, dz, dx in partners(p):
-            d = dz * NX + dx
-            src = block(obuf, place(p, dz, dx))
-            if which == (0, 0, 0, 0):
-                pltpu.make_async_copy(src, block(ret, s), ols.at[0]).start()
+        for q in range(p * PER, (p + 1) * PER):
+            dz, dx = offsets(q)
+            d = ((z + NZ - dz) % NZ) * NX + (x + NX - dx) % NX
+            if q == 0:
+                pltpu.make_async_copy(block(obuf, q), block(ret, s), osem.at[s]).start()
             else:
-                rdma(src, block(ret, s), osem.at[SP], osem.at[s], (d, t)).start()
-
-    def arrive(i, carry):
-        d = (s + i) % SP
-        rdma(block(ret, d), block(ret, d), osem.at[SP], osem.at[d], (s, t)).wait_recv()
+                rdma(block(obuf, q), block(ret, s), osem.at[SP], osem.at[s], (d, t)).start()
+
+    def wave(j, carry):
+        p = j % PIECES
+        stage = j // PIECES - p * DELAY[0] // DELAY[1]
+
+        @pl.when(stage == 0)
+        def _():
+            enter(p)
+
+        @pl.when((stage >= 1) & (stage <= 4))
+        def _():
+            wide.arrivals(stage, p, widen)
+
+        @pl.when(stage == 5)
+        def _():
+            activate(p)
+
+        @pl.when((stage >= 6) & (stage <= 9))
+        def _():
+            deep.arrivals(stage - 5, p, lower)
+
+        for piece in range(PIECES):
+
+            @pl.when((stage == 10) & (p == piece))
+            def _(piece=piece):
+                leave(piece)
+
         return carry
 
-    pltpu.make_async_copy(block(ret, s), block(ret, s), ols.at[0]).wait()
-    lax.fori_loop(1, SP, arrive, 0)
+    lax.fori_loop(0, PIECES * (11 + (PIECES - 1) * DELAY[0] // DELAY[1]), wave, 0)
+
+    def arrive(d, carry):
+        pltpu.make_async_copy(block(ret, d), block(ret, d), osem.at[d]).wait()
+        return carry
+
+    lax.fori_loop(0, SP, arrive, 0)
 
     got0 = jnp.dot(pick0[...], ret[...], preferred_element_type=F32)
     got1 = jnp.dot(pick1[...], ret[...], preferred_element_type=F32)
     routed = got0 * mixw[:, 3:4] + got1 * mixw[:, 4:5]
-    out[...] = (resid[...].astype(F32) + routed).astype(BF16)
+    out[...] = resid[...].astype(F32) + routed
 
     for halo in halos:
         halo.wait_send()
-    branch.drain()
+    rest = bbuf.at[0:15]
+    pltpu.make_async_copy(rest, rest, bss).wait()
     rest = send.at[0 : SLOTS - CAP]
     pltpu.make_async_copy(rest, rest, esem.at[SP]).wait()
     wide.drain()
@@ -397,8 +452,8 @@
         dma((4,)),
         pltpu.VMEM((TP, BROWS, CH), BF16),
         pltpu.VMEM((BROWS, COLS), F32),
-        dma((NY, BPIECES)),
-        dma((NY, BPIECES)),
+        dma((NY, 3)),
+        dma((NY, 3)),
         dma,
         pltpu.VMEM((ROWS, COLS), BF16),
         pltpu.VMEM((SLOTS, ROWS), BF16),
@@ -407,7 +462,6 @@
         pltpu.VMEM((ROWS, CH), F32),
         pltpu.VMEM((SLOTS, COLS), BF16),
         dma((SP + 1,)),
-        dma((1,)),
         pltpu.VMEM((TP, SLOTS, COLS), BF16),
         pltpu.VMEM((SLOTS, 2 * CH), F32),
         pltpu.VMEM((SLOTS, CH), F32),
@@ -422,12 +476,11 @@
         pltpu.VMEM((SLOTS, COLS), BF16),
         pltpu.VMEM((SLOTS, COLS), BF16),
         dma((SP + 1,)),
-        dma((1,)),
     ]
     return pl.pallas_call(
         kernel,
         name="layer",
-        out_shape=jax.ShapeDtypeStruct((ROWS, COLS), BF16),
+        out_shape=jax.ShapeDtypeStruct((ROWS, COLS), F32),
         in_specs=[vmem] * 10 + [hbm] * 4,
         out_specs=vmem,
         scratch_shapes=scratch,
@@ -449,7 +502,7 @@
         gate_weight[0],
         up_weight[0],
         down_weight[0],
-    )
+    ).astype(BF16)
 
 
 def solution(mesh):

time: 128 us -> 121 us (0.945)
  Pallas kernels: 125 us -> 119 us
  other arithmetic: 0 us -> 1.62 us
  local copies, waits for them, and re-layouts: 1.57 us -> 0 us
    pallas_call x1, Pallas kernels: 125 us -> 119 us  [per_device(): pl.pallas_call(kernel, name='layer', out_shape=jax.ShapeDtypeStruct((ROWS...]
    convert_element_type x0 -> x1, other arithmetic: none -> 1.62 us  [per_device(): return pl.pallas_call(kernel, name='layer', out_shape=jax.ShapeDtypeStruc...]
    unnamed x1 -> x0, local copies, waits for them, and re-layouts: 1.57 us -> none
where the time goes in v2:
time: 121 us; the launch traced here: 120 us
  Pallas kernels  119 us (98%)
  other arithmetic  1.62 us (1%)
    pallas_call x1, Pallas kernels, per_device(): pl.pallas_call(kernel, name='layer', out_shape=jax.ShapeDtypeStruct((ROWS...  119 us

profile of v2, /device:TPU:1, one launch (start us, length us, event | category | flops | bytes accessed | tf_op | source)
XLA Modules:
  0.0 120.3 jit_solution(4769258582761456624)
XLA Ops:
  0.0 118.7 %layer.1 = f32[256,256]{1,0:T(8,128)} custom-call(bf16[256,128]{1,0:T(8,128)(2,1)} %og.1, bf16[256,128]{1,0:T(8,128)(2,1)} %ig.1, bf16[256,128]{1,0:T(8,128)(2,1)} %ci.1, bf16[3,128]{1,0:T(4,128)(2,1)} %cw.1, s32[1,256]{1,0:T(1,128)} %bitcast.13, bf16[256,256]{1,0:T(8,128)(2,1)} %resin.1, bf16[2,128]{1,0:T(2,128)(2,1)} %bitcast.15, s32[2,256]{1,0:T(2,128)} %bitcast.11, ...), custom_call_target="tpu_custom_call" | custom-call | tf_op jit(solution)/shard_map/layer/pallas_call | solution.py:480
  118.7 1.6 %convert_element_type.3 = bf16[256,256]{1,0:T(8,128)(2,1)} convert(f32[256,256]{1,0:T(8,128)} %layer.1) | non-fusion elementwise | flops 65536 | bytes 393216 | tf_op jit(solution)/shard_map/convert_element_type | solution.py:505

commit v3 on v2

--- a/solution.py
+++ b/solution.py
@@ -34,9 +34,9 @@
 
 
 class Ring:
-    def __init__(self, buf, pieces, prows, rsem, dsem, ssem, s, y, c):
+    def __init__(self, buf, pieces, prows, rsem, dsem, fsem, ssem, s, y, c):
         self.buf, self.pieces, self.prows = buf, pieces, prows
-        self.rsem, self.dsem, self.ssem = rsem, dsem, ssem
+        self.rsem, self.dsem, self.fsem, self.ssem = rsem, dsem, fsem, ssem
         self.s, self.y, self.c = s, y, c
         self.plus = (s, 2 * ((y + 1) % NY) + c)
         self.minus = (s, 2 * ((y + NY - 1) % NY) + c)
@@ -61,31 +61,38 @@
     def own(self, p, compute):
         compute(2 * self.y + self.c, p)
 
+    def half(self, p, h, dev):
+        rows = self.prows // 2
+        far = self.buf.at[
+            2 * h[0] + self.c, pl.ds(pl.multiple_of(p * self.prows + h[1] * rows, 16), rows)
+        ]
+        return rdma(far, far, self.ssem, self.fsem.at[h[1], p], dev)
+
     def arrivals(self, k, p, compute):
-        low, high = p % 2 == 0, p % 2 == 1
         up = (self.y + NY - k) % NY
         down = (self.y + k) % NY
         c = self.c
 
-        @pl.when((k < 4) | low)
-        def _():
-            self.ring(up, p, self.plus).wait_recv()
-
-            @pl.when((k < 3) | ((k == 3) & low))
-            def _():
-                self.ring(up, p, self.plus).start()
-
+        @pl.when(k < 4)
+        def _():
+            for origin, side, h in ((up, self.plus, 0), (down, self.minus, 1)):
+                self.ring(origin, p, side).wait_recv()
+
+                @pl.when(k < 3)
+                def _():
+                    self.ring(origin, p, side).start()
+
+                @pl.when(k == 3)
+                def _():
+                    self.half(p, (origin, h), side).start()
+
+                self.local(origin, c, p).start()
+
+        @pl.when(k == 4)
+        def _():
+            for h in (0, 1):
+                self.half(p, (up, h), self.plus).wait_recv()
             self.local(up, c, p).start()
-
-        @pl.when((k < 4) | high)
-        def _():
-            self.ring(down, p, self.minus).wait_recv()
-
-            @pl.when((k < 3) | ((k == 3) & high))
-            def _():
-                self.ring(down, p, self.minus).start()
-
-            self.local(down, c, p).start()
 
         compute(2 * up + c, p)
 
@@ -121,8 +128,8 @@
     bbuf, bacc, brs, bds, bss,
     resid, sel, pick0, pick1, mixw,
     send, esem,
-    xbuf, xacc, ssum, xrs, xds, xss,
-    hbuf, hacc, hrs, hds, hss,
+    xbuf, xacc, ssum, xrs, xds, xfs, xss,
+    hbuf, hacc, hrs, hds, hfs, hss,
     obuf, ret, osem,
 ):
     s = lax.axis_index("sp")
@@ -267,13 +274,16 @@
 
     project(6, 5, c)
 
-    def tables(i, carry):
-        rows = pl.ds(pl.multiple_of(i * 256, 256), 256)
-        slot = (lax.broadcasted_iota(jnp.int32, (256, ROWS), 0) + i * 256).astype(F32)
-        sel[rows, :] = jnp.where((slot == slot0) | (slot == slot1), 1.0, 0.0).astype(BF16)
-        return carry
-
-    lax.fori_loop(0, SLOTS // 256, tables, 0)
+    def target(q):
+        dz, dx = ZORDER[q // NX], q % NX
+        return ((z + dz) % NZ) * NX + (x + dx) % NX
+
+    lane_slot = lax.broadcasted_iota(jnp.int32, (CAP, ROWS), 0)
+    for q in range(SP):
+        slot = (lane_slot + target(q) * CAP).astype(F32)
+        sel[q * CAP : (q + 1) * CAP, :] = jnp.where(
+            (slot == slot0) | (slot == slot1), 1.0, 0.0
+        ).astype(BF16)
 
     for off in (3, -3, 4):
         origin = near(off)
@@ -294,26 +304,21 @@
         rows = slice(first, first + size)
         resid[rows, :] = (resin[rows, :].astype(F32) + bacc[lo : lo + size, :]).astype(BF16)
 
-    def group_rows(i, carry):
-        rows = pl.ds(pl.multiple_of(i * 256, 256), 256)
-        send[rows, :] = jnp.dot(sel[rows, :], resid[...], preferred_element_type=F32).astype(BF16)
-        return carry
-
-    lax.fori_loop(0, SLOTS // 256, group_rows, 0)
-
     def block(ref, i):
         return ref.at[pl.ds(pl.multiple_of(i * CAP, CAP), CAP)]
 
     def offsets(q):
         return ZORDER[q // NX], q % NX
 
-    for q in range(SP):
-        dz, dx = offsets(q)
-        d = ((z + dz) % NZ) * NX + (x + dx) % NX
-        if q == 0:
-            pltpu.make_async_copy(block(send, d), block(xbuf.at[t], q), esem.at[q]).start()
-        else:
-            rdma(block(send, d), block(xbuf.at[t], q), esem.at[SP], esem.at[q], (d, t)).start()
+    for p in range(PIECES):
+        rows = slice(p * PROWS, (p + 1) * PROWS)
+        send[rows, :] = jnp.dot(sel[rows, :], resid[...], preferred_element_type=F32).astype(BF16)
+        for q in range(p * PER, (p + 1) * PER):
+            if q == 0:
+                pltpu.make_async_copy(block(send, q), block(xbuf.at[t], q), esem.at[q]).start()
+            else:
+                dev = (target(q), t)
+                rdma(block(send, q), block(xbuf.at[t], q), esem.at[SP], esem.at[q], dev).start()
 
     xacc[...] = jnp.zeros_like(xacc)
     ssum[...] = jnp.zeros_like(ssum)
@@ -343,8 +348,8 @@
     pick0[...] = jnp.where(slot_lane == mixw[:, 1:2], 1.0, 0.0).astype(BF16)
     pick1[...] = jnp.where(slot_lane == mixw[:, 2:3], 1.0, 0.0).astype(BF16)
 
-    wide = Ring(xbuf, PIECES, PROWS, xrs, xds, xss, s, y, c)
-    deep = Ring(hbuf, PIECES, PROWS, hrs, hds, hss, s, y, c)
+    wide = Ring(xbuf, PIECES, PROWS, xrs, xds, xfs, xss, s, y, c)
+    deep = Ring(hbuf, PIECES, PROWS, hrs, hds, hfs, hss, s, y, c)
 
     def enter(p):
         def one(i, carry):
@@ -384,9 +389,9 @@
         p = j % PIECES
         stage = j // PIECES - p * DELAY[0] // DELAY[1]
 
-        @pl.when(stage == 0)
-        def _():
-            enter(p)
+        @pl.when((p == 0) & (j < PIECES * PIECES))
+        def _():
+            enter(j // PIECES)
 
         @pl.when((stage >= 1) & (stage <= 4))
         def _():
@@ -467,11 +472,13 @@
         pltpu.VMEM((SLOTS, CH), F32),
         dma((NY, PIECES)),
         dma((NY, PIECES)),
+        dma((2, PIECES)),
         dma,
         pltpu.VMEM((TP, SLOTS, CH), BF16),
         pltpu.VMEM((SLOTS, COLS), F32),
         dma((NY, PIECES)),
         dma((NY, PIECES)),
+        dma((2, PIECES)),
         dma,
         pltpu.VMEM((SLOTS, COLS), BF16),
         pltpu.VMEM((SLOTS, COLS), BF16),

time: 121 us -> 120 us (level)
  no operation moved by 1% of the time
where the time goes in v3:
time: 120 us
  Pallas kernels  118 us (98%)
  other arithmetic  1.62 us (1%)
    pallas_call x1, Pallas kernels, per_device(): pl.pallas_call(kernel, name='layer', out_shape=jax.ShapeDtypeStruct((ROWS...  118 us

profile of v3, /device:TPU:1, one launch (start us, length us, event | category | flops | bytes accessed | tf_op | source)
XLA Modules:
  0.0 119.7 jit_solution(9966292606338132086)
XLA Ops:
  0.0 118.0 %layer.1 = f32[256,256]{1,0:T(8,128)} custom-call(bf16[256,128]{1,0:T(8,128)(2,1)} %og.1, bf16[256,128]{1,0:T(8,128)(2,1)} %ig.1, bf16[256,128]{1,0:T(8,128)(2,1)} %ci.1, bf16[3,128]{1,0:T(4,128)(2,1)} %cw.1, s32[1,256]{1,0:T(1,128)} %bitcast.13, bf16[256,256]{1,0:T(8,128)(2,1)} %resin.1, bf16[2,128]{1,0:T(2,128)(2,1)} %bitcast.15, s32[2,256]{1,0:T(2,128)} %bitcast.11, ...), custom_call_target="tpu_custom_call" | custom-call | tf_op jit(solution)/shard_map/layer/pallas_call | solution.py:487
  118.1 1.6 %convert_element_type.3 = bf16[256,256]{1,0:T(8,128)(2,1)} convert(f32[256,256]{1,0:T(8,128)} %layer.1) | non-fusion elementwise | flops 65536 | bytes 393216 | tf_op jit(solution)/shard_map/convert_element_type | solution.py:512

commit v4 on v3

--- a/solution.py
+++ b/solution.py
@@ -154,7 +154,7 @@
         return carry
 
     lax.fori_loop(1, SP, greet, 0)
-    for off in (1, 2, NY - 1, NY - 2):
+    for off in range(1, NY):
         peer = 2 * ((y + off) % NY) + c
         pl.semaphore_signal(barrier, inc=1, device_id=(s, peer), device_id_type=MESH)
     pl.semaphore_signal(barrier, inc=1, device_id=(s, 2 * y + 1 - c), device_id_type=MESH)
@@ -209,7 +209,7 @@
     ).astype(BF16)
     bacc[...] = jnp.zeros_like(bacc)
 
-    pl.semaphore_wait(barrier, SP - 1 + 5)
+    pl.semaphore_wait(barrier, SP - 1 + NY)
 
     halos = [
         rdma(ext_p.at[256:264], halo_p, hsem.at[0], hsem.at[1], (nxt, t)),
@@ -232,7 +232,7 @@
         return rdma(ref, ref, bss, bds.at[origin, p], (s, 2 * y + 1 - c))
 
     def open_piece(p):
-        for off in (2, -2, 1, -1):
+        for off in (2, -2, 1, -1) if p < 2 else (4, 3, -3, 2, -2, 1, -1):
             hop(y, p, off).start()
         across(y, c, p).start()
 
@@ -246,15 +246,16 @@
     open_piece(2)
 
     def far_side(p):
-        return 1 if p != 1 else -1
+        return 1 if p == 0 else -1
 
     for p in range(3):
         for side in (1, -1):
             origin = near(-2 * side)
             hop(origin, p, side).wait_recv()
-            if far_side(p) == side:
-                hop(origin, p, 2 * side).start()
-            hop(origin, p, side).start()
+            if p < 2:
+                if far_side(p) == side:
+                    hop(origin, p, 2 * side).start()
+                hop(origin, p, side).start()
             across(origin, c, p).start()
         for side in (1, -1):
             origin = near(-side)

time: 120 us -> 120 us (level)
  no operation moved by 1% of the time
where the time goes in v4:
time: 120 us
  Pallas kernels  118 us (98%)
  other arithmetic  1.62 us (1%)
    pallas_call x1, Pallas kernels, per_device(): pl.pallas_call(kernel, name='layer', out_shape=jax.ShapeDtypeStruct((ROWS...  118 us

profile of v4, /device:TPU:1, one launch (start us, length us, event | category | flops | bytes accessed | tf_op | source)
XLA Modules:
  0.0 119.5 jit_solution(7103269348805332385)
XLA Ops:
  0.0 117.9 %layer.1 = f32[256,256]{1,0:T(8,128)} custom-call(bf16[256,128]{1,0:T(8,128)(2,1)} %og.1, bf16[256,128]{1,0:T(8,128)(2,1)} %ig.1, bf16[256,128]{1,0:T(8,128)(2,1)} %ci.1, bf16[3,128]{1,0:T(4,128)(2,1)} %cw.1, s32[1,256]{1,0:T(1,128)} %bitcast.13, bf16[256,256]{1,0:T(8,128)(2,1)} %resin.1, bf16[2,128]{1,0:T(2,128)(2,1)} %bitcast.15, s32[2,256]{1,0:T(2,128)} %bitcast.11, ...), custom_call_target="tpu_custom_call" | custom-call | tf_op jit(solution)/shard_map/layer/pallas_call | solution.py:488
  117.9 1.6 %convert_element_type.3 = bf16[256,256]{1,0:T(8,128)(2,1)} convert(f32[256,256]{1,0:T(8,128)} %layer.1) | non-fusion elementwise | flops 65536 | bytes 393216 | tf_op jit(solution)/shard_map/convert_element_type | solution.py:513

commit v5 on v4

--- a/solution.py
+++ b/solution.py
@@ -311,10 +311,17 @@
     def offsets(q):
         return ZORDER[q // NX], q % NX
 
+    def hops(q):
+        dz, dx = offsets(q)
+        return min(dz, NZ - dz) + min(dx, NX - dx)
+
+    def far_first(p):
+        return sorted(range(p * PER, (p + 1) * PER), key=lambda q: (-hops(q), q))
+
     for p in range(PIECES):
         rows = slice(p * PROWS, (p + 1) * PROWS)
         send[rows, :] = jnp.dot(sel[rows, :], resid[...], preferred_element_type=F32).astype(BF16)
-        for q in range(p * PER, (p + 1) * PER):
+        for q in far_first(p):
             if q == 0:
                 pltpu.make_async_copy(block(send, q), block(xbuf.at[t], q), esem.at[q]).start()
             else:
@@ -378,7 +385,7 @@
         deep.last(p, lower)
         rows = slice(p * PROWS, (p + 1) * PROWS)
         obuf[rows, :] = hacc[rows, :].astype(BF16)
-        for q in range(p * PER, (p + 1) * PER):
+        for q in far_first(p):
             dz, dx = offsets(q)
             d = ((z + NZ - dz) % NZ) * NX + (x + NX - dx) % NX
             if q == 0:

time: 120 us -> 118 us (0.983)
  Pallas kernels: 118 us -> 116 us
    pallas_call x1, Pallas kernels: 118 us -> 116 us  [per_device(): pl.pallas_call(kernel, name='layer', out_shape=jax.ShapeDtypeStruct((ROWS...]
where the time goes in v5:
time: 118 us
  Pallas kernels  116 us (98%)
  other arithmetic  1.62 us (1%)
    pallas_call x1, Pallas kernels, per_device(): pl.pallas_call(kernel, name='layer', out_shape=jax.ShapeDtypeStruct((ROWS...  116 us

profile of v5, /device:TPU:1, one launch (start us, length us, event | category | flops | bytes accessed | tf_op | source)
XLA Modules:
  0.0 117.9 jit_solution(9137028952315580512)
XLA Ops:
  0.0 116.3 %layer.1 = f32[256,256]{1,0:T(8,128)} custom-call(bf16[256,128]{1,0:T(8,128)(2,1)} %og.1, bf16[256,128]{1,0:T(8,128)(2,1)} %ig.1, bf16[256,128]{1,0:T(8,128)(2,1)} %ci.1, bf16[3,128]{1,0:T(4,128)(2,1)} %cw.1, s32[1,256]{1,0:T(1,128)} %bitcast.13, bf16[256,256]{1,0:T(8,128)(2,1)} %resin.1, bf16[2,128]{1,0:T(2,128)(2,1)} %bitcast.15, s32[2,256]{1,0:T(2,128)} %bitcast.11, ...), custom_call_target="tpu_custom_call" | custom-call | tf_op jit(solution)/shard_map/layer/pallas_call | solution.py:495
  116.3 1.6 %convert_element_type.3 = bf16[256,256]{1,0:T(8,128)(2,1)} convert(f32[256,256]{1,0:T(8,128)} %layer.1) | non-fusion elementwise | flops 65536 | bytes 393216 | tf_op jit(solution)/shard_map/convert_element_type | solution.py:520
